TPU v7x, 32 devices: a whole 2x2x4 slice. The times are simulated.
32 devices in a mesh: ep: 8 (over z, y), tp: 4 (over x, core).
Axes of the slice: x: 2, y: 2, z: 4, core: 2. Of those that a mesh axis runs over, the one named last changes fastest.
Arguments:
- queries: bfloat16 [2048, 1024], P('ep', 'tp'), may hold values from -200 to 200
- keys: bfloat16 [2048, 512], P('ep', 'tp'), may hold values from -5 to 5
- values: bfloat16 [2048, 512], P('ep', 'tp'), may hold values from -6 to 6
- log_gates: float32 [2048, 16], P('ep', 'tp'), may hold values from -2048 to 0, as said below
- out_weight: bfloat16 [1024, 2048], P('tp'), may hold values from -0.1875 to 0.1875
- moe_rows: bfloat16 [2048, 2048], P('ep'), may hold values from -6 to 6
- norm_gain: float32 [2048], replicated, may hold values from 0.1 to 1.9
- experts: int32 [2048, 2], P('ep'), may hold values from 0 to 7, all different within a row; in each aligned block of 256 rows (0 to 255, 256 to 511, ...) at most 128 rows name the same one
- expert_weights: float32 [2048, 2], P('ep'), may hold values from 0.2 to 1
- w_gate: bfloat16 [8, 2048, 1024], P('ep', None, 'tp'), may hold values from -0.125 to 0.125
- w_up: bfloat16 [8, 2048, 1024], P('ep', None, 'tp'), may hold values from -0.125 to 0.125
- w_down: bfloat16 [8, 1024, 2048], P('ep', 'tp'), may hold values from -0.1875 to 0.1875
Outputs:
- mixed: bfloat16 [2048, 2048], P(('ep', 'tp'))
- moe_out: bfloat16 [2048, 2048], P('ep', 'tp')
Inputs may be any that keep to these rules, and one draw needn't show every extreme that they name: Each token names 2 different experts; within the rows of one index of ep (aligned blocks of 256 rows) no expert is named more than 128 times, a bound that some block reaches. `log_gates`: Non-increasing along positions in every head.
All inputs are finite; a program needn't handle non-finite values.
Results may differ from a plain program's by a relative error of at most 0.01195.
Values may be sent and summed in bfloat16 or wider, within the bound.
A program may use at most 128 MiB of HBM per device.

v0:
```python
import math
import jax
import jax.numpy as jnp
from jax import lax
from jax.sharding import PartitionSpec as P

D = 2048
HD = 64
EPSILON = 1e-06
MASKED = -1e30


def prepare_group(query_rows, gate_rows, positions, kv_here, group):
    rows = query_rows.shape[0]
    query_heads = query_rows.reshape(rows, kv_here, group, HD)
    query_gates = jnp.transpose(gate_rows.reshape(rows, kv_here, group), (1, 2, 0))
    return (query_heads, query_gates, positions)


def empty_state(rows, kv_here, group):
    return (
        jnp.full((kv_here, group, rows), MASKED, jnp.float32),
        jnp.zeros((kv_here, group, rows), jnp.float32),
        jnp.zeros((kv_here, group, rows, HD), jnp.float32),
    )


def attend_group(prepared, state, key_part, value_part, gate_part, offset, kv_here, group):
    query_heads, query_gates, query_position = prepared
    length = key_part.shape[0]
    key_span = math.gcd(length, 512)

    def run_blocks(start_state):

        def one_block(turn_index, inner):
            running_max, running_sum, weighted = inner
            first = turn_index * key_span
            key_block = lax.dynamic_slice_in_dim(key_part, first, key_span, 0).reshape(
                key_span, kv_here, HD
            )
            value_block = lax.dynamic_slice_in_dim(value_part, first, key_span, 0).reshape(
                key_span, kv_here, HD
            )
            gate_block = lax.dynamic_slice_in_dim(gate_part, first, key_span, 0).reshape(
                key_span, kv_here, group
            )
            scores = jnp.einsum(
                "qgrd,kgd->grqk", query_heads, key_block, preferred_element_type=jnp.float32
            ) * HD ** (-0.5)
            scores = (
                scores
                + query_gates[..., None]
                - jnp.transpose(gate_block, (1, 2, 0))[:, :, None, :]
            )
            key_position = first + jnp.arange(key_span, dtype=jnp.int32)
            scores = jnp.where(key_position[None, :] <= query_position[:, None], scores, MASKED)
            new_max = jnp.maximum(running_max, jnp.max(scores, axis=-1))
            weights = jnp.exp(scores - new_max[..., None])
            rescale = jnp.exp(running_max - new_max)
            running_sum = running_sum * rescale + jnp.sum(weights, axis=-1)
            weighted = weighted * rescale[..., None] + jnp.einsum(
                "grqk,kgd->grqd",
                weights.astype(jnp.bfloat16),
                value_block,
                preferred_element_type=jnp.float32,
            )
            return (new_max, running_sum, weighted)

        return lax.fori_loop(0, length // key_span, one_block, start_state)

    def keep_state(start_state):
        return start_state

    return lax.cond(offset <= query_position[-1], run_blocks, keep_state, state)


def finish_group(state, heads_here):
    running_max, running_sum, weighted = state
    rows = weighted.shape[2]
    attended = weighted / running_sum[..., None]
    return jnp.transpose(attended, (2, 0, 1, 3)).reshape(rows, heads_here * HD).astype(jnp.bfloat16)


def mixer_half(queries, keys, values, log_gates, out_weight):
    tok_rows = queries.shape[0]
    heads_here = log_gates.shape[1]
    kv_here = keys.shape[1] // HD
    group = heads_here // kv_here
    own_index = lax.axis_index("ep")
    positions = own_index * tok_rows + jnp.arange(tok_rows, dtype=jnp.int32)
    groups = [prepare_group(queries, log_gates, positions, kv_here, group)]
    initial = tuple((empty_state(entry[0].shape[0], kv_here, group) for entry in groups))
    offset = jnp.int32(0)
    key_part = lax.all_gather(keys.astype(jnp.float32), "ep", axis=0, tiled=True).astype(
        jnp.bfloat16
    )
    value_part = lax.all_gather(values.astype(jnp.float32), "ep", axis=0, tiled=True).astype(
        jnp.bfloat16
    )
    gate_part = lax.all_gather(log_gates, "ep", axis=0, tiled=True)
    states = tuple(
        (
            attend_group(
                groups[number],
                initial[number],
                key_part,
                value_part,
                gate_part,
                offset,
                kv_here,
                group,
            )
            for number in range(len(groups))
        )
    )
    finished = [finish_group(state, heads_here) for state in states]
    attended = finished[0]
    return lax.psum_scatter(
        jnp.dot(attended, out_weight, preferred_element_type=jnp.float32).astype(jnp.bfloat16),
        "tp",
        scatter_dimension=0,
        tiled=True,
    )


def experts_half(moe_rows, norm_gain, experts, expert_weights, w_gate, w_up, w_down):
    rows_here = moe_rows.shape[0]
    topk = experts.shape[1]
    experts_all = lax.axis_size("ep")
    capacity = 4 * rows_here // experts_all
    rows_float = moe_rows.astype(jnp.float32)
    normed = (
        rows_float
        * lax.rsqrt(jnp.mean(rows_float * rows_float, axis=-1, keepdims=True) + EPSILON)
        * norm_gain
    ).astype(jnp.bfloat16)
    expert_ids = experts.reshape(-1)
    one_hot = (expert_ids[:, None] == jnp.arange(experts_all, dtype=jnp.int32)[None, :]).astype(
        jnp.int32
    )
    ranks = jnp.cumsum(one_hot, axis=0) - 1
    slot_index = jnp.sum(one_hot * ranks, axis=1)
    destination = expert_ids * capacity + slot_index
    token_index = jnp.arange(rows_here * topk, dtype=jnp.int32) // topk
    width = D // lax.axis_size("tp")
    source_rows = lax.dynamic_slice_in_dim(normed, lax.axis_index("tp") * width, width, 1)
    outgoing = jnp.zeros((experts_all * capacity, source_rows.shape[1]), jnp.bfloat16)
    outgoing = (
        outgoing.at[destination]
        .set(source_rows[token_index])
        .reshape(experts_all, capacity, source_rows.shape[1])
    )
    arrived = lax.all_to_all(outgoing, "ep", split_axis=0, concat_axis=0, tiled=True)
    arrived = lax.all_gather(arrived, "tp", axis=2, tiled=True)
    slots = arrived.shape[1]
    flat_rows = arrived.reshape(-1, D)
    gate_part = jnp.dot(flat_rows, w_gate[0], preferred_element_type=jnp.float32)
    up_part = jnp.dot(flat_rows, w_up[0], preferred_element_type=jnp.float32)
    hidden = (jax.nn.silu(gate_part) * up_part).astype(jnp.bfloat16)
    partial_out = jnp.dot(hidden, w_down[0], preferred_element_type=jnp.float32).reshape(
        experts_all, slots, D
    )
    summed = lax.psum_scatter(
        partial_out.astype(jnp.bfloat16), "tp", scatter_dimension=2, tiled=True
    )
    returned = lax.all_to_all(summed, "ep", split_axis=0, concat_axis=0, tiled=True)
    picked = returned.reshape(experts_all * capacity, -1)[destination].reshape(rows_here, topk, -1)
    return jnp.einsum("tk,tkd->td", expert_weights, picked.astype(jnp.float32)).astype(jnp.bfloat16)


def per_device(
    queries,
    keys,
    values,
    log_gates,
    out_weight,
    moe_rows,
    norm_gain,
    experts,
    expert_weights,
    w_gate,
    w_up,
    w_down,
):
    mixed = mixer_half(queries, keys, values, log_gates, out_weight)
    moe_out = experts_half(moe_rows, norm_gain, experts, expert_weights, w_gate, w_up, w_down)
    return (mixed, moe_out)


def solution(mesh):
    placed = (
        P("ep", "tp"),
        P("ep", "tp"),
        P("ep", "tp"),
        P("ep", "tp"),
        P("tp", None),
        P("ep", None),
        P(),
        P("ep", None),
        P("ep", None),
        P("ep", None, "tp"),
        P("ep", None, "tp"),
        P("ep", "tp", None),
    )
    return jax.shard_map(
        per_device,
        mesh=mesh,
        in_specs=placed,
        out_specs=(P(("ep", "tp"), None), P("ep", "tp")),
        check_vma=False,
    )
```

profile of v0, /device:TPU:0, one launch (start us, length us, event | category | flops | bytes accessed | tf_op | source)
XLA Modules:
  0.0 255.8 jit_solution(16764527390459552446)
XLA Ops:
  7.2 3.0 %convert_element_type.69 = f32[256,2048]{1,0:T(8,128)} convert(bf16[256,2048]{1,0:T(8,128)(2,1)} %param.21) | non-fusion elementwise | flops 524288 | bytes 3145728 | tf_op jit(solution)/shard_map/convert_element_type | solution.py:131
  10.2 0.3 multiply_reduce_fusion
  10.5 0.1 copy.24
  10.6 0.1 eq.29
  10.8 0.1 eq.25
  11.0 1.1 reduce-window.6
  12.1 0.2 slice_reduce_fusion
  12.4 0.1 copy.23
  12.5 0.1 mul.98
  12.7 0.8 dynamic-slice
  13.5 0.1 fusion.18
  13.6 1.2 fusion.14
  14.7 5.0 %scatter_custom_fusion = bf16[1024,512]{1,0:T(8,128)(2,1)S(1)} fusion(s32[512]{0:T(512)S(1)} %bitcast.85, bf16[256,512]{1,0:T(8,128)(2,1)S(1)} %fusion.14, s32[1024]{0:T(1024)S(1)} %pad_clamp_fusion.1, bf16[]{:T(256)} %constant.107.clone.1), kind=kCustom, calls=%fused_computation.35 | custom fusion | bytes 1048578 | tf_op jit(solution)/shard_map/scatter | solution.py:150
  19.8 33.0 %all_to_all.10 = bf16[8,128,512]{2,1,0:T(8,128)(2,1)} all-to-all(bf16[8,128,512]{2,1,0:T(8,128)(2,1)S(1)} %bitcast.78), channel_id=1, replica_groups=mesh['ep'=8,'tp'=4] {'ep'}, dimensions={0} | all-to-all | bytes 2097152 | tf_op jit(solution)/shard_map/all_to_all | solution.py:153
  52.8 0.0 reduce-scatter.5.cloned.1.call-start
  52.9 33.6 %all-gather.2.cloned.1.call-done = bf16[8,128,2048]{2,1,0:T(8,128)(2,1)} async-done(((bf16[8,128,512]{2,1,0:T(8,128)(2,1)}), bf16[8,128,2048]{2,1,0:T(8,128)(2,1)}) %all-gather.2.cloned.1.call-update) | async-done | bytes 4194320 | tf_op jit(solution)/shard_map/all_gather | solution.py:154
  86.4 3.6 %fusion.11 = f32[1024,256]{1,0:T(8,128)S(1)} fusion(bf16[1024,2048]{1,0:T(8,128)(2,1)} %bitcast.91, bf16[1,2048,256]{2,1,0:T(8,128)(2,1)S(1)} %copy-done.9), kind=kOutput, calls=%fused_computation.29 | convolution fusion | flops 1073741824 | bytes 6291456 | tf_op jit(solution)/shard_map/dot_general | solution.py:157
  90.0 0.1 copy-done.10
  90.2 1.3 fusion.8
  91.5 3.2 %convolution_convert_fusion = bf16[8,128,2048]{2,1,0:T(8,128)(2,1)} fusion(bf16[8,128,256]{2,1,0:T(8,128)(2,1)S(1)} %bitcast.81, bf16[1,256,2048]{2,1,0:T(8,128)(2,1)S(1)} %copy-done), kind=kOutput, calls=%fused_computation.22 | convolution fusion | flops 1075838976 | bytes 5767168 | tf_op jit(solution)/shard_map/dot_general | solution.py:160
  94.7 0.0 reduce-scatter.3.cloned.1.call-start
  94.7 0.8 copy-done.3
  95.5 0.1 copy.20
  95.6 0.1 copy.21
  95.8 0.6 slice.9
  97.0 30.7 %all_gather.13 = f32[2048,4]{0,1:T(4,128)S(1)} all-gather(f32[256,4]{0,1:T(4,128)S(1)} %copy-done.5), channel_id=1, replica_groups=mesh['ep'=8,'tp'=4] {'ep'}, dimensions={0}, use_global_device_ids=true | all-gather | bytes 36864 | tf_op jit(solution)/shard_map/all_gather | solution.py:100
  127.7 33.5 %all_gather.12 = bf16[2048,128]{0,1:T(8,128)(2,1)} all-gather(bf16[256,128]{0,1:T(8,128)(2,1)S(1)} %copy.20), channel_id=1, replica_groups=mesh['ep'=8,'tp'=4] {'ep'}, dimensions={0}, use_global_device_ids=true | all-gather | bytes 589824 | tf_op jit(solution)/shard_map/all_gather | solution.py:94
  161.2 33.4 %all_gather.14 = bf16[2048,128]{0,1:T(8,128)(2,1)} all-gather(bf16[256,128]{0,1:T(8,128)(2,1)S(1)} %copy.21), channel_id=1, replica_groups=mesh['ep'=8,'tp'=4] {'ep'}, dimensions={0}, use_global_device_ids=true | all-gather | bytes 589824 | tf_op jit(solution)/shard_map/all_gather | solution.py:97
  194.5 25.2 %conditional.1 = (f32[2,2,256]{2,1,0:T(2,128)}, f32[2,2,256,64]{2,3,1,0:T(8,128)}) conditional(s32[]{:T(128)} %bitcast.1, () %tuple.30, (bf16[256,256]{1,0:T(8,128)(2,1)S(1)}, s32[256]{0:T(256)S(1)}, bf16[2048,128]{0,1:T(8,128)(2,1)}, f32[2,2,256]{2,1,0:T(2,128)S(1)}, f32[2048,4]{0,1:T(4,128)S(1)}, /*index=5*/bf16[2048,128]{0,1:T(8,128)(2,1)}) %tuple.69), branch_computations={%region_0.0_spmd, %region_1.6_spmd} | conditional | flops 139269632 | bytes 8373587 | solution.py:74
  194.5 0.8 copy.22
  195.3 24.4 %while.17 = (s32[]{:T(128)}, f32[2,2,256]{2,1,0:T(2,128)S(1)}, f32[2,2,256]{2,1,0:T(2,128)}, f32[2,2,256,64]{2,3,1,0:T(8,128)}, s32[256]{0:T(256)S(1)}, /*index=...) while((s32[]{:T(128)}, f32[2,2,256]{2,1,0:T(2,128)S(1)}, ...), condition=%wide.region_5.5_spmd.clone, body=%wide.region_2.4_spmd.clone.sunk | while | flops 139269632 | bytes 8111307 | solution.py:69
  195.3 1.0 constant_dynamic-slice_fusion.6
  196.3 0.1 broadcast_compare_fusion.2
  196.5 1.6 fusion.44
  198.1 0.3 fusion.46
  198.4 0.6 fusion.47
  199.0 1.2 convolution_add_fusion.2
  200.2 1.0 constant_dynamic-slice_fusion.6
  201.2 0.1 broadcast_compare_fusion.2
  201.4 1.6 fusion.44
  203.0 0.3 fusion.46
  203.3 1.3 fusion.47
  204.6 2.1 convolution_add_fusion.2
  206.7 1.0 constant_dynamic-slice_fusion.6
  207.7 0.1 broadcast_compare_fusion.2
  207.9 1.6 fusion.44
  209.5 0.3 fusion.46
  209.8 1.3 fusion.47
  211.1 2.1 convolution_add_fusion.2
  213.2 1.0 constant_dynamic-slice_fusion.6
  214.3 0.1 broadcast_compare_fusion.2
  214.4 1.6 fusion.44
  216.0 0.3 fusion.46
  216.3 1.3 fusion.47
  217.6 2.1 convolution_add_fusion.2
  219.7 1.0 divide_convert_fusion
  220.7 2.7 %convolution_convert_fusion.1 = bf16[256,2048]{1,0:T(8,128)(2,1)} fusion(bf16[256,256]{0,1:T(8,128)(2,1)S(1)} %bitcast.80, bf16[256,2048]{1,0:T(8,128)(2,1)} %param.20), kind=kOutput, calls=%fused_computation.23 | convolution fusion | flops 268959744 | bytes 2228224 | tf_op jit(solution)/shard_map/dot_general | solution.py:119
  223.5 5.8 %all-to-all-start.1 = ((bf16[8,128,512]{2,1,0:T(8,128)(2,1)}), bf16[8,128,512]{2,1,0:T(8,128)(2,1)S(1)}, u32[]{:S(2)}, u32[]{:S(2)}) async-start(bf16[8,128,512]{2,1,0:T(8,128)(2,1)} %reduce-scatter.5.cloned.1.call-done), calls=%async_computation.3 | async-start | bytes 2097152 | tf_op jit(solution)/shard_map/all_to_all | solution.py:166
  229.2 0.2 copy.29
  229.4 16.2 %all-to-all-done.1 = bf16[8,128,512]{2,1,0:T(8,128)(2,1)S(1)} async-done(((bf16[8,128,512]{2,1,0:T(8,128)(2,1)}), bf16[8,128,512]{2,1,0:T(8,128)(2,1)S(1)}, u32[]{:S(2)}, u32[]{:S(2)}) %all-to-all-start.1) | async-done | bytes 1048608 | tf_op jit(solution)/shard_map/all_to_all | solution.py:166
  245.6 2.0 gather_fusion
  247.6 0.2 reshape.167
  247.8 0.7 fusion.21
  248.5 0.7 copy.32
  (60 shorter events, 0.4 us)
Async XLA Ops:
  7.2 84.3 %copy-start = (bf16[1,256,2048]{2,1,0:T(8,128)(2,1)S(1)}, bf16[1,256,2048]{2,1,0:T(8,128)(2,1)}, u32[]{:S(2)}) copy-start(bf16[1,256,2048]{2,1,0:T(8,128)(2,1)} %param.27) | copy-start | bytes 3145732
  7.2 3.0 %copy-start.1 = (bf16[256,2048]{1,0:T(8,128)(2,1)S(1)}, bf16[256,2048]{1,0:T(8,128)(2,1)}, u32[]{:S(2)}) copy-start(bf16[256,2048]{1,0:T(8,128)(2,1)} %param.21) | copy-start | bytes 3145732
  7.2 79.2 %all-gather.2.cloned.1.call-start = ((), (), s32[]{:S(2)}) async-start(), calls=%async_computation.5 | async-start | bytes 5242880 | tf_op jit(solution)/shard_map/all_gather | solution.py:154
  7.2 3.3 %copy-start.6 = (s32[256,2]{0,1:T(2,128)S(1)}, s32[256,2]{0,1:T(2,128)}, u32[]{:S(2)}) copy-start(s32[256,2]{0,1:T(2,128)} %param.23) | copy-start | bytes 6148
  14.7 71.7 %copy-start.9 = (bf16[1,2048,256]{2,1,0:T(8,128)(2,1)S(1)}, bf16[1,2048,256]{2,1,0:T(8,128)(2,1)}, u32[]{:S(2)}) copy-start(bf16[1,2048,256]{2,1,0:T(8,128)(2,1)} %param.25) | copy-start | bytes 3145732
  52.8 170.7 %reduce-scatter.5.cloned.1.call-start = ((), (), s32[]{:S(2)}) async-start(), calls=%async_computation.6 | async-start | bytes 5242880 | tf_op jit(solution)/shard_map/reduce_scatter | solution.py:163
  86.4 3.6 %copy-start.8 = (bf16[8,128,2048]{2,1,0:T(8,128)(2,1)S(1)}, bf16[8,128,2048]{2,1,0:T(8,128)(2,1)}, u32[]{:S(2)}) copy-start(bf16[8,128,2048]{2,1,0:T(8,128)(2,1)} %all-gather.2.cloned.1.call-done) | copy-start | bytes 12582916
  86.4 3.7 %copy-start.10 = (bf16[1,2048,256]{2,1,0:T(8,128)(2,1)S(1)}, bf16[1,2048,256]{2,1,0:T(8,128)(2,1)}, u32[]{:S(2)}) copy-start(bf16[1,2048,256]{2,1,0:T(8,128)(2,1)} %param.26) | copy-start | bytes 3145732
  94.7 0.8 copy-start.3
  94.7 1.0 copy-start.4
  94.7 1.1 copy-start.5
  94.7 99.9 %copy-start.2 = (bf16[256,256]{1,0:T(8,128)(2,1)S(1)}, bf16[256,256]{1,0:T(8,128)(2,1)}, u32[]{:S(2)}) copy-start(bf16[256,256]{1,0:T(8,128)(2,1)} %param.16) | copy-start | bytes 393220
  94.7 154.6 %reduce-scatter.3.cloned.1.call-start = ((), (), s32[]{:S(2)}) async-start(), calls=%async_computation.4 | async-start | bytes 1310720 | tf_op jit(solution)/shard_map/reduce_scatter | solution.py:118
  223.4 5.8 %copy-start.7 = (f32[256,2]{0,1:T(2,128)S(1)}, f32[256,2]{0,1:T(2,128)}, u32[]{:S(2)}) copy-start(f32[256,2]{0,1:T(2,128)} %param.24) | copy-start | bytes 6148
  223.5 22.2 %all-to-all-start.1 = ((bf16[8,128,512]{2,1,0:T(8,128)(2,1)}), bf16[8,128,512]{2,1,0:T(8,128)(2,1)S(1)}, u32[]{:S(2)}, u32[]{:S(2)}) async-start(bf16[8,128,512]{2,1,0:T(8,128)(2,1)} %reduce-scatter.5.cloned.1.call-done), calls=%async_computation.3 | async-start | bytes 2097152 | tf_op jit(solution)/shard_map/all_to_all | solution.py:166
Sparse Core Ops, SparseCore 0:
  52.9 33.4 all-gather.1
  94.8 44.3 reduce-scatter.4
  223.6 25.0 reduce-scatter.2
where the time goes:
time: 257 us; the launch traced here: 256 us
  blocking collectives  131 us (51%)
  waiting for transfers between devices  49.8 us (19%)
  matrix products  25.3 us (10%)
  local copies, waits for them, and re-layouts  16.4 us (6%)
  between operations  14.7 us (6%)
  other arithmetic  13 us (5%)
  starting transfers between devices  5.88 us (2%)
    all_gather x1, waiting for transfers between devices, experts_half(): arrived = lax.all_gather(arrived, 'tp', axis=2, tiled=True)  33.6 us
    all_gather x1, blocking collectives, mixer_half(): lax.all_gather(keys.astype(jnp.float32), 'ep', axis=0, tiled=True)  33.5 us
    all_gather x1, blocking collectives, mixer_half(): lax.all_gather(values.astype(jnp.float32), 'ep', axis=0, tiled=True)  33.4 us
    all_to_all x1, blocking collectives, experts_half(): lax.all_to_all(outgoing, 'ep', split_axis=0, concat_axis=0, tiled=True)  33 us
    all_gather x1, blocking collectives, mixer_half(): gate_part = lax.all_gather(log_gates, 'ep', axis=0, tiled=True)  30.7 us
    all_to_all x1, waiting for transfers between devices, experts_half(): lax.all_to_all(summed, 'ep', split_axis=0, concat_axis=0, tiled=True)  16.2 us
    dot_general x4, matrix products, one_block(): jnp.einsum('grqk,kgd->grqd', weights.astype(jnp.bfloat16), value_block, p...  7.5 us
    dot_general x4, matrix products, one_block(): jnp.einsum('qgrd,kgd->grqk', query_heads, key_block, preferred_element_ty...  6.37 us
  transfers between devices with their start and end apart: 4, of which 2 were waited for; matrix products, arithmetic and copies ran while one was open for 13% of the time, Pallas kernels for 0%

commit v1 on v0

--- a/solution.py
+++ b/solution.py
@@ -1,3 +1,4 @@
+import functools
 import math
 import jax
 import jax.numpy as jnp
@@ -8,6 +9,35 @@
 HD = 64
 EPSILON = 1e-06
 MASKED = -1e30
+
+
+def roots_proceed(my_tile, d_out, raw):
+    spare, current_arr = (my_tile.shape[:d_out], my_tile.shape[d_out + 1 :])
+    return jnp.moveaxis(my_tile.reshape(*spare, raw, -1, *current_arr), d_out, 0)
+
+
+def turn_sides(x_part, in_dim):
+    t_next = list(x_part.shape[1:])
+    t_next[in_dim] *= x_part.shape[0]
+    return jnp.moveaxis(x_part, 0, in_dim).reshape(t_next)
+
+
+def supply_sample(array_in, peer_axis, matrix, z):
+    aux = lax.axis_size(peer_axis)
+    mid_arr, v_now = (aux, lax.axis_index(peer_axis))
+    e_next = roots_proceed(array_in, matrix, mid_arr)
+    blocks_here = [e_next[v_now]]
+    for at in [*range(1, mid_arr)]:
+        u_next = e_next[(v_now + at) % mid_arr]
+        state_next = lax.ppermute(
+            u_next, peer_axis, [(dev_j, (dev_j + at) % mid_arr) for dev_j in range(mid_arr)]
+        )
+        blocks_here.append(state_next)
+    e_next = jnp.stack(blocks_here)[(v_now - jnp.arange(mid_arr)) % mid_arr]
+    return turn_sides(e_next, z)
+
+
+bench_refer = functools.partial(supply_sample, peer_axis="ep", matrix=0, z=0)
 
 
 def prepare_group(query_rows, gate_rows, positions, kv_here, group):
@@ -150,7 +180,7 @@
         .set(source_rows[token_index])
         .reshape(experts_all, capacity, source_rows.shape[1])
     )
-    arrived = lax.all_to_all(outgoing, "ep", split_axis=0, concat_axis=0, tiled=True)
+    arrived = bench_refer(outgoing)
     arrived = lax.all_gather(arrived, "tp", axis=2, tiled=True)
     slots = arrived.shape[1]
     flat_rows = arrived.reshape(-1, D)

time: 257 us -> 255 us (level)
  blocking collectives: 131 us -> 97.5 us
  waiting for transfers between devices: 49.8 us -> 65.1 us
  starting transfers between devices: 5.88 us -> 20.3 us
    all_to_all x1 -> x0, blocking collectives: 33 us -> none  [experts_half(): lax.all_to_all(outgoing, 'ep', split_axis=0, concat_axis=0, tiled=True)]
    ppermute x0 -> x7, starting transfers between devices: none -> 14.4 us  [supply_sample(): lax.ppermute(u_next, peer_axis, [(dev_j, (dev_j + at) % mid_arr) for dev_...]
    all_gather x1, waiting for transfers between devices: 33.6 us -> 42 us  [experts_half(): arrived = lax.all_gather(arrived, 'tp', axis=2, tiled=True)]
    ppermute x0 -> x7, waiting for transfers between devices: none -> 6.81 us  [supply_sample(): lax.ppermute(u_next, peer_axis, [(dev_j, (dev_j + at) % mid_arr) for dev_...]
  transfers between devices with their start and end apart: 4 -> 11, of which waited for: 2 -> 4; matrix products, arithmetic and copies ran while one was open for 13% -> 13% of each run, Pallas kernels for 0% -> 0%
where the time goes in v1:
time: 255 us; the launch traced here: 254 us
  blocking collectives  97.5 us (38%)
  waiting for transfers between devices  65.1 us (26%)
  matrix products  25.3 us (10%)
  starting transfers between devices  20.3 us (8%)
  local copies, waits for them, and re-layouts  18.1 us (7%)
  between operations  14.9 us (6%)
  other arithmetic  13 us (5%)
    all_gather x1, waiting for transfers between devices, experts_half(): arrived = lax.all_gather(arrived, 'tp', axis=2, tiled=True)  42 us
    all_gather x1, blocking collectives, mixer_half(): lax.all_gather(keys.astype(jnp.float32), 'ep', axis=0, tiled=True)  33.5 us
    all_gather x1, blocking collectives, mixer_half(): lax.all_gather(values.astype(jnp.float32), 'ep', axis=0, tiled=True)  33.4 us
    all_gather x1, blocking collectives, mixer_half(): gate_part = lax.all_gather(log_gates, 'ep', axis=0, tiled=True)  30.7 us
    all_to_all x1, waiting for transfers between devices, experts_half(): lax.all_to_all(summed, 'ep', split_axis=0, concat_axis=0, tiled=True)  16.2 us
    ppermute x7, starting transfers between devices, supply_sample(): lax.ppermute(u_next, peer_axis, [(dev_j, (dev_j + at) % mid_arr) for dev_...  14.4 us
    dot_general x4, matrix products, one_block(): jnp.einsum('grqk,kgd->grqd', weights.astype(jnp.bfloat16), value_block, p...  7.48 us
    ppermute x7, waiting for transfers between devices, supply_sample(): lax.ppermute(u_next, peer_axis, [(dev_j, (dev_j + at) % mid_arr) for dev_...  6.81 us
  transfers between devices with their start and end apart: 11, of which 4 were waited for; matrix products, arithmetic and copies ran while one was open for 13% of the time, Pallas kernels for 0%

profile of v1, /device:TPU:0, one launch (start us, length us, event | category | flops | bytes accessed | tf_op | source)
XLA Modules:
  0.0 254.3 jit_solution(12733820807935180615)
XLA Ops:
  7.3 2.9 %convert_element_type.69 = f32[256,2048]{1,0:T(8,128)} convert(bf16[256,2048]{1,0:T(8,128)(2,1)} %param.21) | non-fusion elementwise | flops 524288 | bytes 3145728 | tf_op jit(solution)/shard_map/convert_element_type | solution.py:161
  10.3 0.3 multiply_reduce_fusion
  10.7 0.1 eq.39
  11.0 1.1 reduce-window.6
  12.2 0.2 slice_reduce_fusion
  12.6 0.1 mul.98
  12.9 0.8 dynamic-slice
  13.7 1.1 fusion.14
  14.8 5.0 %scatter_custom_fusion = bf16[1024,512]{1,0:T(8,128)(2,1)S(1)} fusion(s32[512]{0:T(512)S(1)} %bitcast.117, bf16[256,512]{1,0:T(8,128)(2,1)S(1)} %fusion.14, s32[1024]{0:T(1024)S(1)} %pad_clamp_fusion.2, bf16[]{:T(256)} %constant.157.clone.1), kind=kCustom, calls=%fused_computation.36 | custom fusion | bytes 1048578 | tf_op jit(solution)/shard_map/scatter | solution.py:180
  20.0 3.0 %collective-permute-start = (bf16[1,128,512]{2,1,0:T(8,128)(2,1)S(1)}, bf16[1,128,512]{2,1,0:T(8,128)(2,1)S(1)}, u32[]{:S(2)}, u32[]{:S(2)}) collective-permute-start(bf16[1,128,512]{2,1,0:T(8,128)(2,1)S(1)} %get-tuple-element.274), channel_id=1, source_target_pairs={{0,4},{4,8},{8,12},{12,16},{16,20},{20,24},{24,28},{28,0},{1,5},{5... | collective-permute-start | bytes 393224 | tf_op jit(solution)/shard_map/ppermute | solution.py:32
  23.1 1.6 collective-permute-start.1
  24.6 2.5 collective-permute-start.2
  27.2 1.2 collective-permute-start.3
  28.4 2.6 %collective-permute-start.4 = (bf16[1,128,512]{2,1,0:T(8,128)(2,1)S(1)}, bf16[1,128,512]{2,1,0:T(8,128)(2,1)S(1)}, u32[]{:S(2)}, u32[]{:S(2)}) collective-permute-start(bf16[1,128,512]{2,1,0:T(8,128)(2,1)S(1)} %get-tuple-element.270), channel_id=1, source_target_pairs={{0,20},{4,24},{8,28},{12,0},{16,4},{20,8},{24,12},{28,16},{1,21},{... | collective-permute-start | bytes 393224 | tf_op jit(solution)/shard_map/ppermute | solution.py:32
  31.1 1.4 collective-permute-start.5
  32.5 2.0 collective-permute-start.6
  34.5 6.5 %collective-permute-done.2 = bf16[1,128,512]{2,1,0:T(8,128)(2,1)S(1)} collective-permute-done((bf16[1,128,512]{2,1,0:T(8,128)(2,1)S(1)}, bf16[1,128,512]{2,1,0:T(8,128)(2,1)S(1)}, u32[]{:S(2)}, u32[]{:S(2)}) %collective-permute-start.2) | collective-permute-done | bytes 131104 | tf_op jit(solution)/shard_map/ppermute | solution.py:32
  41.0 0.3 collective-permute-done.3
  41.4 1.6 gather_fusion
  43.0 42.0 %all-gather.3.cloned.1.call-done = bf16[8,128,2048]{2,1,0:T(8,128)(2,1)} async-done(((bf16[8,128,512]{2,1,0:T(8,128)(2,1)}), bf16[8,128,2048]{2,1,0:T(8,128)(2,1)}) %all-gather.3.cloned.1.call-update) | async-done | bytes 4194320 | tf_op jit(solution)/shard_map/all_gather | solution.py:184
  85.0 3.6 %fusion.11 = f32[1024,256]{1,0:T(8,128)S(1)} fusion(bf16[1024,2048]{1,0:T(8,128)(2,1)} %bitcast.123, bf16[1,2048,256]{2,1,0:T(8,128)(2,1)S(1)} %copy-done.9), kind=kOutput, calls=%fused_computation.30 | convolution fusion | flops 1073741824 | bytes 6291456 | tf_op jit(solution)/shard_map/dot_general | solution.py:187
  88.8 1.3 fusion.8
  90.1 3.2 %convolution_convert_fusion = bf16[8,128,2048]{2,1,0:T(8,128)(2,1)} fusion(bf16[8,128,256]{2,1,0:T(8,128)(2,1)S(1)} %bitcast.113, bf16[1,256,2048]{2,1,0:T(8,128)(2,1)S(1)} %copy-done), kind=kOutput, calls=%fused_computation.23 | convolution fusion | flops 1075838976 | bytes 5767168 | tf_op jit(solution)/shard_map/dot_general | solution.py:190
  93.4 0.8 copy-done.3
  94.4 0.6 slice.9
  95.6 30.7 %all_gather.13 = f32[2048,4]{0,1:T(4,128)S(1)} all-gather(f32[256,4]{0,1:T(4,128)S(1)} %copy-done.5), channel_id=1, replica_groups=mesh['ep'=8,'tp'=4] {'ep'}, dimensions={0}, use_global_device_ids=true | all-gather | bytes 36864 | tf_op jit(solution)/shard_map/all_gather | solution.py:130
  126.3 33.5 %all_gather.12 = bf16[2048,128]{0,1:T(8,128)(2,1)} all-gather(bf16[256,128]{0,1:T(8,128)(2,1)S(1)} %copy.20), channel_id=1, replica_groups=mesh['ep'=8,'tp'=4] {'ep'}, dimensions={0}, use_global_device_ids=true | all-gather | bytes 589824 | tf_op jit(solution)/shard_map/all_gather | solution.py:124
  159.8 33.4 %all_gather.14 = bf16[2048,128]{0,1:T(8,128)(2,1)} all-gather(bf16[256,128]{0,1:T(8,128)(2,1)S(1)} %copy.21), channel_id=1, replica_groups=mesh['ep'=8,'tp'=4] {'ep'}, dimensions={0}, use_global_device_ids=true | all-gather | bytes 589824 | tf_op jit(solution)/shard_map/all_gather | solution.py:127
  193.2 25.1 %conditional.1 = (f32[2,2,256]{2,1,0:T(2,128)}, f32[2,2,256,64]{2,3,1,0:T(8,128)}) conditional(s32[]{:T(128)} %bitcast.1, () %tuple.30, (bf16[256,256]{1,0:T(8,128)(2,1)S(1)}, s32[256]{0:T(256)S(1)}, bf16[2048,128]{0,1:T(8,128)(2,1)}, f32[2,2,256]{2,1,0:T(2,128)S(1)}, f32[2048,4]{0,1:T(4,128)S(1)}, /*index=5*/bf16[2048,128]{0,1:T(8,128)(2,1)}) %tuple.77), branch_computations={%region_0.0_spmd, %region_1.6_spmd} | conditional | flops 139269632 | bytes 8373587 | solution.py:104
  193.2 0.8 copy.22
  193.9 24.4 %while.17 = (s32[]{:T(128)}, f32[2,2,256]{2,1,0:T(2,128)S(1)}, f32[2,2,256]{2,1,0:T(2,128)}, f32[2,2,256,64]{2,3,1,0:T(8,128)}, s32[256]{0:T(256)S(1)}, /*index=...) while((s32[]{:T(128)}, f32[2,2,256]{2,1,0:T(2,128)S(1)}, ...), condition=%wide.region_5.5_spmd.clone, body=%wide.region_2.4_spmd.clone.sunk | while | flops 139269632 | bytes 8111307 | solution.py:99
  193.9 1.0 constant_dynamic-slice_fusion.6
  195.0 0.1 broadcast_compare_fusion.2
  195.1 1.6 fusion.46
  196.7 0.3 fusion.48
  197.0 0.6 fusion.49
  197.6 1.2 convolution_add_fusion.2
  198.8 1.0 constant_dynamic-slice_fusion.6
  199.8 0.1 broadcast_compare_fusion.2
  200.0 1.6 fusion.46
  201.6 0.3 fusion.48
  201.9 1.3 fusion.49
  203.2 2.1 convolution_add_fusion.2
  205.3 1.0 constant_dynamic-slice_fusion.6
  206.4 0.1 broadcast_compare_fusion.2
  206.5 1.6 fusion.46
  208.1 0.3 fusion.48
  208.4 1.3 fusion.49
  209.7 2.1 convolution_add_fusion.2
  211.8 1.0 constant_dynamic-slice_fusion.6
  212.9 0.1 broadcast_compare_fusion.2
  213.0 1.6 fusion.46
  214.6 0.3 fusion.48
  214.9 1.3 fusion.49
  216.2 2.1 convolution_add_fusion.2
  218.3 1.0 divide_convert_fusion
  219.3 2.7 %convolution_convert_fusion.1 = bf16[256,2048]{1,0:T(8,128)(2,1)} fusion(bf16[256,256]{0,1:T(8,128)(2,1)S(1)} %bitcast.112, bf16[256,2048]{1,0:T(8,128)(2,1)} %param.20), kind=kOutput, calls=%fused_computation.24 | convolution fusion | flops 268959744 | bytes 2228224 | tf_op jit(solution)/shard_map/dot_general | solution.py:149
  222.0 5.8 %all-to-all-start = ((bf16[8,128,512]{2,1,0:T(8,128)(2,1)}), bf16[8,128,512]{2,1,0:T(8,128)(2,1)S(1)}, u32[]{:S(2)}, u32[]{:S(2)}) async-start(bf16[8,128,512]{2,1,0:T(8,128)(2,1)} %reduce-scatter.5.cloned.1.call-done), calls=%async_computation.2 | async-start | bytes 2097152 | tf_op jit(solution)/shard_map/all_to_all | solution.py:196
  227.8 0.2 copy.29
  228.0 16.2 %all-to-all-done = bf16[8,128,512]{2,1,0:T(8,128)(2,1)S(1)} async-done(((bf16[8,128,512]{2,1,0:T(8,128)(2,1)}), bf16[8,128,512]{2,1,0:T(8,128)(2,1)S(1)}, u32[]{:S(2)}, u32[]{:S(2)}) %all-to-all-start) | async-done | bytes 1048608 | tf_op jit(solution)/shard_map/all_to_all | solution.py:196
  244.2 2.0 gather_fusion.1
  246.2 0.2 reshape.216
  246.4 0.7 fusion.23
  247.1 0.7 copy.32
  (83 shorter events, 1.6 us)
Async XLA Ops:
  7.2 82.9 %copy-start = (bf16[1,256,2048]{2,1,0:T(8,128)(2,1)S(1)}, bf16[1,256,2048]{2,1,0:T(8,128)(2,1)}, u32[]{:S(2)}) copy-start(bf16[1,256,2048]{2,1,0:T(8,128)(2,1)} %param.27) | copy-start | bytes 3145732
  7.2 3.1 %copy-start.1 = (bf16[256,2048]{1,0:T(8,128)(2,1)S(1)}, bf16[256,2048]{1,0:T(8,128)(2,1)}, u32[]{:S(2)}) copy-start(bf16[256,2048]{1,0:T(8,128)(2,1)} %param.21) | copy-start | bytes 3145732
  7.2 77.8 %all-gather.3.cloned.1.call-start = ((), (), s32[]{:S(2)}) async-start(), calls=%async_computation.5 | async-start | bytes 5242880 | tf_op jit(solution)/shard_map/all_gather | solution.py:184
  7.3 3.2 %copy-start.6 = (s32[256,2]{0,1:T(2,128)S(1)}, s32[256,2]{0,1:T(2,128)}, u32[]{:S(2)}) copy-start(s32[256,2]{0,1:T(2,128)} %param.23) | copy-start | bytes 6148
  20.0 11.1 %collective-permute-start = (bf16[1,128,512]{2,1,0:T(8,128)(2,1)S(1)}, bf16[1,128,512]{2,1,0:T(8,128)(2,1)S(1)}, u32[]{:S(2)}, u32[]{:S(2)}) collective-permute-start(bf16[1,128,512]{2,1,0:T(8,128)(2,1)S(1)} %get-tuple-element.274), channel_id=1, source_target_pairs={{0,4},{4,8},{8,12},{12,16},{16,20},{20,24},{24,28},{28,0},{1,5},{5... | collective-permute-start | bytes 393224 | tf_op jit(solution)/shard_map/ppermute | solution.py:32
  23.1 9.4 %collective-permute-start.1 = (bf16[1,128,512]{2,1,0:T(8,128)(2,1)S(1)}, bf16[1,128,512]{2,1,0:T(8,128)(2,1)S(1)}, u32[]{:S(2)}, u32[]{:S(2)}) collective-permute-start(bf16[1,128,512]{2,1,0:T(8,128)(2,1)S(1)} %get-tuple-element.273), channel_id=1, source_target_pairs={{0,8},{4,12},{8,16},{12,20},{16,24},{20,28},{24,0},{28,4},{1,9},{5... | collective-permute-start | bytes 393224 | tf_op jit(solution)/shard_map/ppermute | solution.py:32
  24.6 16.3 %collective-permute-start.2 = (bf16[1,128,512]{2,1,0:T(8,128)(2,1)S(1)}, bf16[1,128,512]{2,1,0:T(8,128)(2,1)S(1)}, u32[]{:S(2)}, u32[]{:S(2)}) collective-permute-start(bf16[1,128,512]{2,1,0:T(8,128)(2,1)S(1)} %get-tuple-element.272), channel_id=1, source_target_pairs={{0,12},{4,16},{8,20},{12,24},{16,28},{20,0},{24,4},{28,8},{1,13},{... | collective-permute-start | bytes 393224 | tf_op jit(solution)/shard_map/ppermute | solution.py:32
  27.2 14.1 %collective-permute-start.3 = (bf16[1,128,512]{2,1,0:T(8,128)(2,1)S(1)}, bf16[1,128,512]{2,1,0:T(8,128)(2,1)S(1)}, u32[]{:S(2)}, u32[]{:S(2)}) collective-permute-start(bf16[1,128,512]{2,1,0:T(8,128)(2,1)S(1)} %get-tuple-element.271), channel_id=1, source_target_pairs={{0,16},{4,20},{8,24},{12,28},{16,0},{20,4},{24,8},{28,12},{1,17},{... | collective-permute-start | bytes 393224 | tf_op jit(solution)/shard_map/ppermute | solution.py:32
  28.4 12.9 %collective-permute-start.4 = (bf16[1,128,512]{2,1,0:T(8,128)(2,1)S(1)}, bf16[1,128,512]{2,1,0:T(8,128)(2,1)S(1)}, u32[]{:S(2)}, u32[]{:S(2)}) collective-permute-start(bf16[1,128,512]{2,1,0:T(8,128)(2,1)S(1)} %get-tuple-element.270), channel_id=1, source_target_pairs={{0,20},{4,24},{8,28},{12,0},{16,4},{20,8},{24,12},{28,16},{1,21},{... | collective-permute-start | bytes 393224 | tf_op jit(solution)/shard_map/ppermute | solution.py:32
  31.1 10.3 %collective-permute-start.5 = (bf16[1,128,512]{2,1,0:T(8,128)(2,1)S(1)}, bf16[1,128,512]{2,1,0:T(8,128)(2,1)S(1)}, u32[]{:S(2)}, u32[]{:S(2)}) collective-permute-start(bf16[1,128,512]{2,1,0:T(8,128)(2,1)S(1)} %get-tuple-element.269), channel_id=1, source_target_pairs={{0,24},{4,28},{8,0},{12,4},{16,8},{20,12},{24,16},{28,20},{1,25},{... | collective-permute-start | bytes 393224 | tf_op jit(solution)/shard_map/ppermute | solution.py:32
  32.5 8.9 %collective-permute-start.6 = (bf16[1,128,512]{2,1,0:T(8,128)(2,1)S(1)}, bf16[1,128,512]{2,1,0:T(8,128)(2,1)S(1)}, u32[]{:S(2)}, u32[]{:S(2)}) collective-permute-start(bf16[1,128,512]{2,1,0:T(8,128)(2,1)S(1)} %get-tuple-element.268), channel_id=1, source_target_pairs={{0,28},{4,0},{8,4},{12,8},{16,12},{20,16},{24,20},{28,24},{1,29},{... | collective-permute-start | bytes 393224 | tf_op jit(solution)/shard_map/ppermute | solution.py:32
  41.0 44.1 %copy-start.9 = (bf16[1,2048,256]{2,1,0:T(8,128)(2,1)S(1)}, bf16[1,2048,256]{2,1,0:T(8,128)(2,1)}, u32[]{:S(2)}) copy-start(bf16[1,2048,256]{2,1,0:T(8,128)(2,1)} %param.25) | copy-start | bytes 3145732
  43.0 179.0 %reduce-scatter.5.cloned.1.call-start = ((), (), s32[]{:S(2)}) async-start(), calls=%async_computation.4 | async-start | bytes 5242880 | tf_op jit(solution)/shard_map/reduce_scatter | solution.py:193
  85.0 3.6 %copy-start.8 = (bf16[8,128,2048]{2,1,0:T(8,128)(2,1)S(1)}, bf16[8,128,2048]{2,1,0:T(8,128)(2,1)}, u32[]{:S(2)}) copy-start(bf16[8,128,2048]{2,1,0:T(8,128)(2,1)} %all-gather.3.cloned.1.call-done) | copy-start | bytes 12582916
  85.0 3.7 %copy-start.10 = (bf16[1,2048,256]{2,1,0:T(8,128)(2,1)S(1)}, bf16[1,2048,256]{2,1,0:T(8,128)(2,1)}, u32[]{:S(2)}) copy-start(bf16[1,2048,256]{2,1,0:T(8,128)(2,1)} %param.26) | copy-start | bytes 3145732
  93.3 0.8 copy-start.3
  93.3 1.0 copy-start.4
  93.3 1.1 copy-start.5
  93.3 99.9 %copy-start.2 = (bf16[256,256]{1,0:T(8,128)(2,1)S(1)}, bf16[256,256]{1,0:T(8,128)(2,1)}, u32[]{:S(2)}) copy-start(bf16[256,256]{1,0:T(8,128)(2,1)} %param.16) | copy-start | bytes 393220
  93.3 154.5 %reduce-scatter.3.cloned.1.call-start = ((), (), s32[]{:S(2)}) async-start(), calls=%async_computation.3 | async-start | bytes 1310720 | tf_op jit(solution)/shard_map/reduce_scatter | solution.py:148
  222.0 5.8 %copy-start.7 = (f32[256,2]{0,1:T(2,128)S(1)}, f32[256,2]{0,1:T(2,128)}, u32[]{:S(2)}) copy-start(f32[256,2]{0,1:T(2,128)} %param.24) | copy-start | bytes 6148
  222.0 22.2 %all-to-all-start = ((bf16[8,128,512]{2,1,0:T(8,128)(2,1)}), bf16[8,128,512]{2,1,0:T(8,128)(2,1)S(1)}, u32[]{:S(2)}, u32[]{:S(2)}) async-start(bf16[8,128,512]{2,1,0:T(8,128)(2,1)} %reduce-scatter.5.cloned.1.call-done), calls=%async_computation.2 | async-start | bytes 2097152 | tf_op jit(solution)/shard_map/all_to_all | solution.py:196
Sparse Core Ops, SparseCore 0:
  43.1 41.8 all-gather.2
  93.4 44.3 reduce-scatter.4
  222.1 25.0 reduce-scatter.2
